TPU v7x, 256 devices: a whole 4x4x8 slice. The times are simulated.
256 devices in a mesh: gr: 2 (over z_hi), sp: 16 (over z_lo, y), tp: 8 (over x, core).
Axes of the slice: x: 4, y: 4, z: 8 (z_hi: 2, z_lo: 4; z = z_hi * 4 + z_lo), core: 2. Of those that a mesh axis runs over, the one named last changes fastest.
Arguments:
- tokens: bfloat16 [8, 8, 2048, 4096], P('gr', 'tp', 'sp'), may hold values from -6 to 6
- ln_gain: bfloat16 [4096], replicated, may hold values from 0.099609375 to 1.8984375
- w_key: bfloat16 [4096, 256], P('sp'), may hold values from -0.09375 to 0.09375
- w_value: bfloat16 [4096, 256], P('sp'), may hold values from -0.09375 to 0.09375
- queries: bfloat16 [32, 512], P(('gr', 'sp')), may hold values from -6 to 6
- head_shift: float32 [4, 8], replicated
- key_shift: float32 [32, 16384], P(('gr', 'sp'), 'tp')
Outputs:
- kv_cache: bfloat16 [32, 16384, 128], P(('gr', 'sp'), 'tp')
- first_read: float32 [32, 512], P(('gr', 'sp'))
All inputs are finite; a program needn't handle non-finite values.
Results may differ from a plain program's by a relative error of at most 0.0064.
Values may be sent and summed in bfloat16 or wider, within the bound.
A program may use at most 64 MiB of HBM per device.

v0:
```python
import math

import jax
import jax.numpy as jnp
from jax import lax
from jax.sharding import Mesh
from jax.sharding import PartitionSpec as P

HD = 64
KVH = 4
GROUP = 8
SP = ("sp_0", "sp_1")
GR_SP = ("gr", "sp_0", "sp_1")


epsilon = 1e-05


def in_order(pieces, dim):
    pieces = jnp.moveaxis(pieces, 0, dim)
    shape = pieces.shape
    return pieces.reshape(*shape[:dim], shape[dim] * shape[dim + 1], *shape[dim + 2 :])


def stacked_from(shard, axes, sequence):
    pieces = shard[None]
    for k in sequence:
        pieces = lax.all_gather(pieces, axes[k], axis=0, tiled=True)
    carried = [lax.axis_size(axes[k]) for k in reversed(sequence)]
    pieces = pieces.reshape(*carried, *shard.shape)
    turned = sorted(range(len(sequence)), key=lambda place: sequence[len(sequence) - 1 - place])
    return pieces.transpose(*turned, *range(len(sequence), pieces.ndim)).reshape(-1, *shard.shape)


def whole_of(shard, axes, sequence, dim):
    return in_order(stacked_from(shard, axes, sequence), dim)


def side_by_side(arrays, axis, dim, along):
    widths = [math.prod(a.shape[along:]) for a in arrays]
    both = jnp.concatenate(
        [a.reshape(*a.shape[:along], w) for a, w in zip(arrays, widths)], axis=along
    )
    filled = lax.all_gather(both, axis, axis=dim, tiled=True)
    pieces = jnp.split(filled, [sum(widths[:k]) for k in range(1, len(widths))], axis=along)
    return tuple(
        (b.reshape(*filled.shape[:along], *a.shape[along:]) for a, b in zip(arrays, pieces))
    )


def add_columns(normed, segment):
    return jnp.dot(normed, segment, preferred_element_type=jnp.float32)


def local(tokens, ln_gain, w_key, w_value, queries, head_shift, key_shift):
    seq_count = tokens.shape[0]
    sub_count = tokens.shape[2]
    width = tokens.shape[3]
    flat_rows = tokens.reshape(seq_count * sub_count, width).astype(jnp.float32)
    row_mean = jnp.mean(flat_rows, axis=1, keepdims=True)
    centred = flat_rows - row_mean
    row_var = jnp.mean(centred * centred, axis=1, keepdims=True)
    normed = (centred * lax.rsqrt(row_var + epsilon) * ln_gain.astype(jnp.float32)).astype(
        jnp.bfloat16
    )
    keys = add_columns(normed, whole_of(w_key, SP, (0, 1), 0))
    values = add_columns(normed, whole_of(w_value, SP, (0, 1), 0))
    joined = jnp.concatenate(
        [
            keys.astype(jnp.bfloat16).reshape(seq_count, sub_count, KVH, HD),
            values.astype(jnp.bfloat16).reshape(seq_count, sub_count, KVH, HD),
        ],
        axis=3,
    )
    arranged = jnp.transpose(joined, (0, 2, 1, 3)).reshape(seq_count * KVH, sub_count, 2 * HD)
    cache_here = lax.all_to_all(arranged, SP, split_axis=0, concat_axis=1, tiled=True)
    own_keys = cache_here[0, :, :HD]
    own_values = cache_here[0, :, HD:]
    kv_head = lax.axis_index(SP) % KVH
    picker = (jnp.arange(KVH) == kv_head).astype(jnp.float32)
    head_row = jnp.sum(picker[:, None] * head_shift, axis=0)
    query = queries.reshape(GROUP, HD)
    logits = jnp.einsum("gd,jd->gj", query, own_keys, preferred_element_type=jnp.float32) * HD ** (
        -0.5
    )
    logits = logits + head_row[:, None] + key_shift[0][None, :]
    log_beta = jax.nn.log_sigmoid(logits)
    log_keep = log_beta - logits
    within = lax.cumsum(log_keep, axis=1, reverse=True) - log_keep
    local_weight = jnp.exp(log_beta + within).astype(jnp.bfloat16)
    section_part = jnp.dot(local_weight, own_values, preferred_element_type=jnp.float32)
    section_total = jnp.sum(log_keep, axis=1)
    all_totals, all_parts = side_by_side((section_total[None], section_part[None]), "tp", 0, 2)
    carry_all = lax.cumsum(all_totals, axis=0, reverse=True) - all_totals
    first_read = jnp.sum(jnp.exp(carry_all)[:, :, None] * all_parts, axis=0)
    return (cache_here, first_read.reshape(1, GROUP * HD))


def solution(mesh):
    split = Mesh(
        mesh.devices.reshape(mesh.shape["gr"], 4, 4, mesh.shape["tp"]), ("gr", "sp_0", "sp_1", "tp")
    )
    placed = (
        P("gr", "tp", SP, None),
        P(),
        P(SP, None),
        P(SP, None),
        P(GR_SP, None),
        P(),
        P(GR_SP, "tp"),
    )
    return jax.shard_map(
        local,
        mesh=split,
        in_specs=placed,
        out_specs=(P(GR_SP, "tp", None), P(GR_SP, None)),
        check_vma=False,
    )
```

profile of v0, /device:TPU:1, one launch (start us, length us, event | category | flops | bytes accessed | tf_op | source)
XLA Modules:
  0.0 156.6 jit_solution(1758660517415116715)
XLA Ops:
  7.2 0.0 all-gather.7.cloned.1.call-start
  7.2 17.0 %all-gather.1 = bf16[1024,256]{1,0:T(8,128)(2,1)} all-gather(bf16[256,256]{1,0:T(8,128)(2,1)} %param.10), channel_id=3, replica_groups=mesh['gr'=2,'sp_0'=4,'sp_1'=4,'tp'=8] {'sp_0'}, dimensions={0}, use_global_device_ids=true | all-gather | bytes 655360 | tf_op jit(solution)/shard_map/all_gather | solution.py:28
  24.2 0.0 all-gather.7.cloned.1.call-update
  24.3 0.0 all-gather.5.cloned.1.call-start
  24.3 13.4 %all-gather = bf16[1024,256]{1,0:T(8,128)(2,1)} all-gather(bf16[256,256]{1,0:T(8,128)(2,1)} %param.9), channel_id=2, replica_groups=mesh['gr'=2,'sp_0'=4,'sp_1'=4,'tp'=8] {'sp_0'}, dimensions={0}, use_global_device_ids=true | all-gather | bytes 655360 | tf_op jit(solution)/shard_map/all_gather | solution.py:28
  37.7 0.0 all-gather.5.cloned.1.call-update
  37.8 0.0 copy-start
  37.8 0.9 convert_element_type.34
  38.6 3.4 %convert_reduce_fusion = f32[4,128]{1,0:T(4,128)S(1)} fusion(bf16[4,1,128,4096]{3,2,1,0:T(8,128)(2,1)} %param.7), kind=kLoop, calls=%fused_computation.1 | loop fusion | flops 4193792 | bytes 4196352 | tf_op jit(solution)/shard_map/reduce_sum | solution.py:60
  42.1 0.0 copy-done
  42.1 1.2 fusion.2
  43.3 4.3 %fusion.4 = bf16[4,1,128,4096]{3,2,1,0:T(8,128)(2,1)} fusion(bf16[4,1,128,4096]{3,2,1,0:T(8,128)(2,1)S(1)} %copy-done, f32[4096]{0:T(1024)S(1)} %convert_element_type.34, f32[4,128]{1,0:T(4,128)S(1)} %add_rsqrt_fusion, f32[4,128]{1,0:T(4,128)S(1)} %broadcast_multiply_fusion), kind=kLoop, calls=%fused_computation.6 | loop fusion | flops 10485760 | bytes 8409088 | tf_op jit(solution)/shard_map/convert_element_type | solution.py:63
  47.6 12.9 %all-gather.7.cloned.1.call-done = bf16[16,256,256]{2,1,0:T(8,128)(2,1)} async-done(((bf16[4,256,256]{2,1,0:T(8,128)(2,1)}), bf16[16,256,256]{2,1,0:T(8,128)(2,1)}) %all-gather.7.cloned.1.call-update) | async-done | bytes 2097168 | tf_op jit(solution)/shard_map/all_gather | solution.py:28
  60.6 0.0 copy-start.1
  60.6 1.9 %copy.25 = bf16[4,4,256,256]{3,2,1,0:T(8,128)(2,1)S(1)} copy(bf16[4,4,256,256]{3,2,0,1:T(8,128)(2,1)} %bitcast.57) | data formatting | bytes 4194304 | tf_op jit(solution)/shard_map/transpose | solution.py:32
  62.4 0.9 copy-done.1
  63.4 1.2 convolution_convert_fusion
  64.6 0.1 copy.26
  64.8 0.1 reshape.121
  64.8 30.9 %all-gather.5.cloned.1.call-done = bf16[16,256,256]{2,1,0:T(8,128)(2,1)} async-done(((bf16[4,256,256]{2,1,0:T(8,128)(2,1)}), bf16[16,256,256]{2,1,0:T(8,128)(2,1)}) %all-gather.5.cloned.1.call-update) | async-done | bytes 2097168 | tf_op jit(solution)/shard_map/all_gather | solution.py:28
  95.8 0.0 copy-start.2
  95.8 1.9 %copy.23 = bf16[4,4,256,256]{3,2,1,0:T(8,128)(2,1)S(1)} copy(bf16[4,4,256,256]{3,2,0,1:T(8,128)(2,1)} %bitcast.56) | data formatting | bytes 4194304 | tf_op jit(solution)/shard_map/transpose | solution.py:32
  97.7 0.9 copy-done.2
  98.6 0.0 copy-start.3
  98.6 0.0 copy-start.4
  98.6 0.0 copy-start.5
  98.6 1.2 convolution_convert_fusion.1
  99.9 0.1 copy.24
  100.0 0.1 reshape.119
  100.1 0.3 maximum_bitcast_fusion
  100.4 1.1 copy.27
  101.5 5.8 %all-to-all-start = ((bf16[16,128,128]{2,1,0:T(8,128)(2,1)}), bf16[16,128,128]{2,1,0:T(8,128)(2,1)S(1)}, u32[]{:S(2)}, u32[]{:S(2)}) async-start(bf16[16,128,128]{2,1,0:T(8,128)(2,1)} %bitcast.10), calls=%async_computation | async-start | bytes 1048576 | tf_op jit(solution)/shard_map/all_to_all | solution.py:76
  107.4 0.0 copy-done.3
  107.4 0.1 reshape.123
  107.5 0.0 copy-done.4
  107.5 0.1 multiply_reduce_fusion
  107.6 13.4 %all-to-all-done = bf16[16,128,128]{2,1,0:T(8,128)(2,1)S(1)} async-done(((bf16[16,128,128]{2,1,0:T(8,128)(2,1)}), bf16[16,128,128]{2,1,0:T(8,128)(2,1)S(1)}, u32[]{:S(2)}, u32[]{:S(2)}) %all-to-all-start) | async-done | bytes 524320 | tf_op jit(solution)/shard_map/all_to_all | solution.py:76
  121.0 0.0 copy-done.5
  121.0 0.2 fusion.7
  121.3 0.2 fusion.18
  121.5 9.9 %reduce-window.6 = f32[8,16,128]{2,1,0:T(8,128)S(1)} reduce-window(f32[8,16,128]{2,1,0:T(8,128)S(1)} %copy.28, f32[]{:T(128)} %constant.30.clone.1), window={size=1x1x128 pad=0_0x0_0x0_127}, to_apply=%region_4.5 | reduce-window | flops 2080768 | bytes 131076 | tf_op jit(solution)/shard_map/reduce-window
  131.4 0.1 slice_reduce_fusion
  131.5 0.2 reduce-window.9
  131.7 0.1 slice.14
  131.8 0.1 add_bitcast_fusion
  131.8 0.3 convolution_bitcast_fusion
  132.2 0.1 copy.29
  132.3 0.1 pad_maximum_fusion
  132.3 15.7 %all_gather.19 = f32[8,8,65]{2,1,0:T(8,128)S(1)} all-gather(f32[1,8,65]{2,1,0:T(8,128)S(1)} %pad_maximum_fusion), channel_id=1, replica_groups=mesh['gr'=2,'sp_0'=4,'sp_1'=4,'tp'=8] {'tp'}, dimensions={0}, use_global_device_ids=true | all-gather | bytes 18720 | tf_op jit(solution)/shard_map/all_gather | solution.py:44
  148.0 0.1 copy.31
  148.2 0.1 fusion.14
  148.3 0.7 reshape.126
  149.0 0.8 copy.36
  (7 shorter events, 0.1 us)
Async XLA Ops:
  7.2 53.4 %all-gather.7.cloned.1.call-start = ((), (), s32[]{:S(2)}) async-start(), calls=%async_computation.2 | async-start | bytes 2621440 | tf_op jit(solution)/shard_map/all_gather | solution.py:28
  24.3 71.5 %all-gather.5.cloned.1.call-start = ((), (), s32[]{:S(2)}) async-start(), calls=%async_computation.1 | async-start | bytes 2621440 | tf_op jit(solution)/shard_map/all_gather | solution.py:28
  37.8 4.3 %copy-start = (bf16[4,1,128,4096]{3,2,1,0:T(8,128)(2,1)S(1)}, bf16[4,1,128,4096]{3,2,1,0:T(8,128)(2,1)}, u32[]{:S(2)}) copy-start(bf16[4,1,128,4096]{3,2,1,0:T(8,128)(2,1)} %param.7) | copy-start | bytes 12582916
  60.6 2.8 %copy-start.1 = (bf16[4,1,128,4096]{3,2,1,0:T(8,128)(2,1)S(1)}, bf16[4,1,128,4096]{3,2,1,0:T(8,128)(2,1)}, u32[]{:S(2)}) copy-start(bf16[4,1,128,4096]{3,2,1,0:T(8,128)(2,1)} %fusion.4) | copy-start | bytes 12582916
  95.8 2.8 %copy-start.2 = (bf16[4,1,128,4096]{3,2,1,0:T(8,128)(2,1)S(1)}, bf16[4,1,128,4096]{3,2,1,0:T(8,128)(2,1)}, u32[]{:S(2)}) copy-start(bf16[4,1,128,4096]{3,2,1,0:T(8,128)(2,1)} %fusion.4) | copy-start | bytes 12582916
  98.6 8.8 %copy-start.3 = (bf16[1,512]{1,0:T(2,128)(2,1)S(1)}, bf16[1,512]{1,0:T(2,128)(2,1)}, u32[]{:S(2)}) copy-start(bf16[1,512]{1,0:T(2,128)(2,1)} %param.11) | copy-start | bytes 3076
  98.6 8.9 %copy-start.4 = (f32[4,8]{1,0:T(4,128)S(1)}, f32[4,8]{1,0:T(4,128)}, u32[]{:S(2)}) copy-start(f32[4,8]{1,0:T(4,128)} %param.12) | copy-start | bytes 388
  98.6 22.4 %copy-start.5 = (f32[1,2048]{1,0:T(1,128)S(1)}, f32[1,2048]{1,0:T(1,128)}, u32[]{:S(2)}) copy-start(f32[1,2048]{1,0:T(1,128)} %param.13) | copy-start | bytes 24580
  101.5 19.5 %all-to-all-start = ((bf16[16,128,128]{2,1,0:T(8,128)(2,1)}), bf16[16,128,128]{2,1,0:T(8,128)(2,1)S(1)}, u32[]{:S(2)}, u32[]{:S(2)}) async-start(bf16[16,128,128]{2,1,0:T(8,128)(2,1)} %bitcast.10), calls=%async_computation | async-start | bytes 1048576 | tf_op jit(solution)/shard_map/all_to_all | solution.py:76
Sparse Core Ops, SparseCore 0:
  24.4 36.1 all-gather.6
  62.4 33.3 all-gather.4
where the time goes:
time: 157 us
  waiting for transfers between devices  57.3 us (36%)
  blocking collectives  46.2 us (29%)
  other arithmetic  20.9 us (13%)
  between operations  14.2 us (9%)
  local copies, waits for them, and re-layouts  9.08 us (6%)
  starting transfers between devices  5.9 us (4%)
  matrix products  3.04 us (2%)
    all_gather x2, waiting for transfers between devices, stacked_from(): pieces = lax.all_gather(pieces, axes[k], axis=0, tiled=True)  43.9 us
    all_gather x2, blocking collectives, stacked_from(): pieces = lax.all_gather(pieces, axes[k], axis=0, tiled=True)  30.5 us
    all_gather x1, blocking collectives, side_by_side(): filled = lax.all_gather(both, axis, axis=dim, tiled=True)  15.7 us
    all_to_all x1, waiting for transfers between devices, local(): lax.all_to_all(arranged, SP, split_axis=0, concat_axis=1, tiled=True)  13.4 us
    another operation x2, other arithmetic  10.1 us
    all_to_all x1, starting transfers between devices, local(): lax.all_to_all(arranged, SP, split_axis=0, concat_axis=1, tiled=True)  5.82 us
    convert_element_type x1, other arithmetic, local(): (centred * lax.rsqrt(row_var + epsilon) * ln_gain.astype(jnp.float32)).as...  4.3 us
    transpose x2, local copies, waits for them, and re-layouts, stacked_from(): pieces.transpose(*turned, *range(len(sequence), pieces.ndim))  3.76 us
  transfers between devices with their start and end apart: 3, of which 3 were waited for; matrix products, arithmetic and copies ran while one was open for 9% of the time, Pallas kernels for 0%

commit v1 on v0

v1 whole, which is shorter than its diff:
```python
import functools

import jax
import jax.numpy as jnp
from jax import lax
from jax.experimental import pallas as pl
from jax.experimental.pallas import tpu as pltpu
from jax.sharding import PartitionSpec as P

MESH = pl.DeviceIdType.MESH
F32, BF16 = jnp.float32, jnp.bfloat16
D, HD, KVH, GROUP = 4096, 64, 4, 8
EPS = 1e-05
SPLIT = ((128, 128, 0), (0, 0, 256))
MAX_COPIES = 112


def kernel(
    tok_hbm, gain_hbm, wk_hbm, wv_hbm, q_hbm, hs_hbm, ks_hbm,
    cache_hbm, read_hbm,
    tok, nrm, w, acc, kvs, kvr, cache, gain, qv, hsv, ksv, rdv, xs, xr,
    local_sem, send_sem, recv_sem,
):
    gr, sp, tp = lax.axis_index("gr"), lax.axis_index("sp"), lax.axis_index("tp")
    x, core = tp // 2, tp % 2
    zl, y = sp // 4, sp % 4
    z = gr * 4 + zl

    def at_z(k):
        far = (z + k) % 8
        return (far // 4, (far % 4) * 4 + y, tp)

    def at_y(k):
        return (gr, zl * 4 + (y + k) % 4, tp)

    def at_x(k):
        return (gr, sp, ((x + k) % 4) * 2 + core)

    def at_sp(k):
        return (gr, (sp + k) % 16, tp)

    def at_tp(k):
        return (gr, sp, (tp + k) % 8)

    sibling = (gr, sp, x * 2 + 1 - core)

    copies = []

    def send(src, dst, device):
        number = len(copies)
        copy = pltpu.make_async_remote_copy(
            src_ref=src,
            dst_ref=dst,
            send_sem=send_sem.at[number],
            recv_sem=recv_sem.at[number],
            device_id=device,
            device_id_type=MESH,
        )
        copy.start()
        copies.append(copy)
        return copy

    locals_ = []

    def fetch(src, dst):
        copy = pltpu.make_async_copy(src, dst, local_sem.at[len(locals_)])
        copy.start()
        locals_.append(copy)
        return copy

    plan = []
    for c in range(2):
        a, b, d = SPLIT[c]
        p = {"c": c, "a": a // 2, "b": b // 2, "d": d // 8}
        p["a0"] = pl.multiple_of(core * (a // 2), 32)
        p["b0"] = pl.multiple_of(a + core * (b // 2), 32)
        p["d0"] = pl.multiple_of(a + b + tp * (d // 8), 16)
        p["own"] = []
        for size in ("a", "b", "d"):
            if p[size]:
                rows = pl.ds(p[size + "0"], p[size])
                source = (wk_hbm, wv_hbm)[c].at[rows, :]
                p["own"].append(fetch(source, w.at[c, zl, y, rows, :]))
        plan.append(p)
    got_gain = fetch(gain_hbm, gain)
    got_tok = [fetch(tok_hbm.at[s, 0], tok.at[s]) for s in range(4)]
    got_small = [fetch(q_hbm, qv), fetch(hs_hbm, hsv), fetch(ks_hbm, ksv)]

    barrier = pltpu.get_barrier_semaphore()
    friends = [at_z(k) for k in (1, -1, 2, -2)]
    friends += [at_sp(k) for k in range(1, 16)]
    friends += [at_tp(k) for k in range(1, 8)]
    for friend in friends:
        pl.semaphore_signal(barrier, inc=1, device_id=friend, device_id_type=MESH)
    pl.semaphore_wait(barrier, len(friends))

    def piece(c, zi, yi, start, count):
        return w.at[c, zi, yi, pl.ds(start, count), :]

    def both(c, zi, yi, start, count, device):
        ref = piece(c, zi, yi, start, count)
        return send(ref, ref, device)

    every = pl.ds(0, 4)
    low, high = pl.ds(0, 2), pl.ds(2, 2)

    def stage1(p):
        c = p["c"]
        p["s1"] = []
        if p["a"]:
            for k in (1, -1, 2 - 4 * core):
                p["s1"].append(both(c, zl, y, p["a0"], p["a"], at_z(k)))
        if p["b"]:
            for k in (1, -1, 2):
                p["s1"].append(both(c, zl, y, p["b0"], p["b"], at_y(k)))
        if p["d"]:
            for k in range(1, 16):
                p["s1"].append(both(c, zl, y, p["d0"], p["d"], at_sp(k)))

    def stage2(p):
        c = p["c"]
        for copy in p["s1"]:
            copy.wait_recv()
        p["s2"], p["pair"] = [], []
        if p["a"]:
            for k in (1, -1):
                p["s2"].append(both(c, every, y, p["a0"], p["a"], at_y(k)))
        if p["b"]:
            for k in (1, -1):
                p["s2"].append(both(c, zl, every, p["b0"], p["b"], at_z(k)))
        if p["d"]:
            for k in (1, -1):
                p["s2"].append(both(c, every, every, p["d0"], p["d"], at_x(k)))
        if p["a"]:
            p["pair"].append(both(c, every, y, p["a0"], p["a"], sibling))
        if p["b"]:
            p["pair"].append(both(c, zl, every, p["b0"], p["b"], sibling))
        if p["d"]:
            p["pair"].append(both(c, every, every, p["d0"], p["d"], sibling))

    def stage3(p):
        c = p["c"]
        for copy in p["s2"]:
            copy.wait_recv()
        p["s3"] = []
        up, down = (y + 1) % 4, (y + 3) % 4
        zup, zdown = (zl + 1) % 4, (zl + 3) % 4
        xup, xdown = (x + 1) % 4, (x + 3) % 4
        if p["a"]:
            p["s3"].append(both(c, low, down, p["a0"], p["a"], at_y(1)))
            p["s3"].append(both(c, high, up, p["a0"], p["a"], at_y(-1)))
        if p["b"]:
            p["s3"].append(both(c, zdown, low, p["b0"], p["b"], at_z(1)))
            p["s3"].append(both(c, zup, high, p["b0"], p["b"], at_z(-1)))
        if p["d"]:
            base = p["d0"] - tp * p["d"]
            first = pl.multiple_of(base + (xdown * 2 + core) * p["d"], 16)
            second = pl.multiple_of(base + (xup * 2 + core) * p["d"], 16)
            p["s3"].append(both(c, low, every, first, p["d"], at_x(1)))
            p["s3"].append(both(c, high, every, second, p["d"], at_x(-1)))
        if p["a"]:
            for side in (down, up):
                p["pair"].append(both(c, every, side, p["a0"], p["a"], sibling))
        if p["b"]:
            for side in (zdown, zup):
                p["pair"].append(both(c, side, every, p["b0"], p["b"], sibling))
        if p["d"]:
            for start in (first, second):
                p["pair"].append(both(c, every, every, start, p["d"], sibling))

    def stage4(p):
        c = p["c"]
        for copy in p["s3"]:
            copy.wait_recv()
        if p["a"]:
            p["pair"].append(both(c, every, (y + 2) % 4, p["a0"], p["a"], sibling))
        if p["b"]:
            p["pair"].append(both(c, (zl + 2) % 4, every, p["b0"], p["b"], sibling))
        if p["d"]:
            base = p["d0"] - tp * p["d"]
            start = pl.multiple_of(base + (((x + 2) % 4) * 2 + core) * p["d"], 16)
            p["pair"].append(both(c, every, every, start, p["d"], sibling))

    def stage5(p):
        for copy in p["pair"]:
            copy.wait_recv()

    def norm(s):
        got_tok[s].wait()

        def block(i, carry):
            for half in range(2):
                r = pl.multiple_of(i * 32 + half * 16, 16)
                rows = pl.ds(r, 16)
                tile = lambda j: tok[s, rows, j * 128 : (j + 1) * 128].astype(F32)
                sums = [tile(j) for j in range(4)]
                for j in range(4, 32):
                    sums[j % 4] = sums[j % 4] + tile(j)
                total = (sums[0] + sums[1]) + (sums[2] + sums[3])
                mean = jnp.sum(total, axis=1, keepdims=True) * (1.0 / D)
                squares = [None] * 4
                for j in range(32):
                    gap = tile(j) - mean
                    old = squares[j % 4]
                    squares[j % 4] = gap * gap if old is None else old + gap * gap
                total = (squares[0] + squares[1]) + (squares[2] + squares[3])
                var = jnp.sum(total, axis=1, keepdims=True) * (1.0 / D)
                scale = lax.rsqrt(var + EPS)
                out_rows = pl.ds(pl.multiple_of(s * 128 + r, 16), 16)
                for j in range(32):
                    cols = slice(j * 128, (j + 1) * 128)
                    value = (tile(j) - mean) * scale * gain[:, cols].astype(F32)
                    nrm[out_rows, cols] = value.astype(BF16)
            return carry

        lax.fori_loop(0, 4, block, 0)

    lane = lax.broadcasted_iota(jnp.int32, (64, 128), 1)
    left = lane < HD
    left8 = left[:8]

    def turn(v):
        return pltpu.roll(v, HD, 1)

    def project(c):
        acc[...] = jnp.dot(
            nrm[...], w[c].reshape(D, 256), preferred_element_type=F32
        )
        for s in range(4):
            for p in range(2):
                cols = slice(p * 128, (p + 1) * 128)
                top = acc[s * 128 : s * 128 + 64, cols]
                bottom = acc[s * 128 + 64 : s * 128 + 128, cols]
                even = jnp.where(left, top, turn(bottom))
                odd = jnp.where(left, turn(top), bottom)
                kvs[c, s * 4 + 2 * p] = even.astype(BF16)
                kvs[c, s * 4 + 2 * p + 1] = odd.astype(BF16)
        kvr[c, sp] = kvs[c, sp]
        out = []
        for k in range(1, 16):
            far = at_sp(k)
            out.append(send(kvs.at[c, far[1]], kvr.at[c, sp], far))
        return out

    for p in plan:
        for copy in p["own"]:
            copy.wait()
    stage1(plan[0])
    stage1(plan[1])
    got_gain.wait()
    norm(0)
    stage2(plan[0])
    norm(1)
    stage2(plan[1])
    norm(2)
    stage3(plan[0])
    norm(3)
    stage4(plan[0])
    stage3(plan[1])
    stage5(plan[0])
    moved_k = project(0)
    stage4(plan[1])
    stage5(plan[1])
    moved_v = project(1)

    for copy in got_small:
        copy.wait()
    row8 = lax.broadcasted_iota(jnp.int32, (8, 128), 0)
    qq = jnp.zeros((8, 128), F32)
    for g in range(GROUP):
        part = qv[:, (g // 2) * 128 : (g // 2 + 1) * 128].astype(F32)
        part = jnp.broadcast_to(part, (8, 128))
        other = turn(part)
        mine = jnp.where(left8, part, other) if g % 2 == 0 else jnp.where(left8, other, part)
        qq = jnp.where(row8 == g, mine, qq)
    q_lo = jnp.where(left8, qq, 0.0)
    q_hi = jnp.where(left8, 0.0, qq)
    stack = jnp.concatenate([q_lo, q_hi], axis=0).astype(BF16)
    hrow = lax.broadcasted_iota(jnp.int32, (4, 8), 0)
    own = jnp.sum(jnp.where(hrow == y, hsv[...], 0.0), axis=0, keepdims=True)
    eye = lax.broadcasted_iota(jnp.int32, (8, 8), 0) == lax.broadcasted_iota(jnp.int32, (8, 8), 1)
    head = jnp.sum(jnp.where(eye, jnp.broadcast_to(own, (8, 8)), 0.0), axis=1, keepdims=True)

    for copy in moved_k:
        copy.wait_recv()
    logits = lax.dot_general(
        stack, kvr[0].reshape(1024, 128), (((1,), (1,)), ((), ())), preferred_element_type=F32
    )
    tiles = []
    for m in range(8):
        cols = slice(m * 128, (m + 1) * 128)
        lo, hi = logits[:8, cols], logits[8:, cols]
        tiles.append(jnp.where(left8, lo, turn(hi)))
        tiles.append(jnp.where(left8, turn(lo), hi))
    z_all = jnp.concatenate(
        [
            t * HD ** (-0.5) + head + ksv[:, n * 128 : (n + 1) * 128]
            for n, t in enumerate(tiles)
        ],
        axis=0,
    )
    log_beta = jnp.minimum(z_all, 0.0) - jnp.log1p(jnp.exp(-jnp.abs(z_all)))
    log_keep = log_beta - z_all
    ri = lax.broadcasted_iota(jnp.int32, (128, 256), 0)
    ci = lax.broadcasted_iota(jnp.int32, (128, 256), 1)
    later = jnp.where((ci >= 128) | (ri > ci), 1.0, 0.0).astype(F32)
    sums = jnp.dot(
        log_keep, later, preferred_element_type=F32, precision=lax.Precision.HIGHEST
    )
    tail = jnp.zeros((8, 128), F32)
    weights = [None] * 16
    for n in reversed(range(16)):
        rows = slice(n * 8, (n + 1) * 8)
        weights[n] = jnp.exp(log_beta[rows] + (sums[rows, :128] + tail))
        tail = tail + sums[rows, 128:]
    w_lo = [jnp.where(left8, weights[2 * m], turn(weights[2 * m + 1])) for m in range(8)]
    w_hi = [jnp.where(left8, turn(weights[2 * m]), weights[2 * m + 1]) for m in range(8)]
    wstack = jnp.concatenate(
        [jnp.concatenate(w_lo, axis=1), jnp.concatenate(w_hi, axis=1)], axis=0
    ).astype(BF16)

    for copy in moved_v:
        copy.wait_recv()
    out = jnp.dot(wstack, kvr[1].reshape(1024, 128), preferred_element_type=F32)
    section = out[:8] + turn(out[8:])
    message = jnp.where(left8, section, tail)
    xs[...] = message
    xr[tp] = message
    shared = [send(xs, xr.at[tp], at_tp(k)) for k in range(1, 8)]

    def assemble(j, carry):
        keys = kvr[0, j].astype(F32)
        values = kvr[1, j].astype(F32)
        first = pl.multiple_of(j * 128, 64)
        second = pl.multiple_of(j * 128 + 64, 64)
        cache[pl.ds(first, 64), :] = jnp.where(left, keys, turn(values)).astype(BF16)
        cache[pl.ds(second, 64), :] = jnp.where(left, turn(keys), values).astype(BF16)
        return carry

    lax.fori_loop(0, 16, assemble, 0)
    stored = fetch(cache, cache_hbm.at[0])

    for copy in shared:
        copy.wait_recv()
    carry = jnp.zeros((8, 128), F32)
    result = jnp.zeros((8, 128), F32)
    for t in reversed(range(8)):
        tile = xr[t]
        result = result + jnp.exp(carry) * tile
        carry = carry + turn(tile)
    result = jnp.where(left8, result, turn(result))
    for k in range(4):
        rdv[:, k * 128 : (k + 1) * 128] = jnp.where(
            left8[:1], result[2 * k : 2 * k + 1], result[2 * k + 1 : 2 * k + 2]
        )
    answered = fetch(rdv, read_hbm)
    for copy in copies:
        copy.wait_send()
    stored.wait()
    answered.wait()


def local(tokens, ln_gain, w_key, w_value, queries, head_shift, key_shift):
    any_ = pl.BlockSpec(memory_space=pl.ANY)
    return pl.pallas_call(
        kernel,
        out_shape=(
            jax.ShapeDtypeStruct((1, 2048, 128), BF16),
            jax.ShapeDtypeStruct((1, 512), F32),
        ),
        in_specs=[any_] * 7,
        out_specs=(any_, any_),
        scratch_shapes=[
            pltpu.VMEM((4, 128, D), BF16),
            pltpu.VMEM((512, D), BF16),
            pltpu.VMEM((2, 4, 4, 256, 256), BF16),
            pltpu.VMEM((512, 256), F32),
            pltpu.VMEM((2, 16, 64, 128), BF16),
            pltpu.VMEM((2, 16, 64, 128), BF16),
            pltpu.VMEM((2048, 128), BF16),
            pltpu.VMEM((1, D), BF16),
            pltpu.VMEM((1, 512), BF16),
            pltpu.VMEM((4, 8), F32),
            pltpu.VMEM((1, 2048), F32),
            pltpu.VMEM((1, 512), F32),
            pltpu.VMEM((8, 128), F32),
            pltpu.VMEM((8, 8, 128), F32),
            pltpu.SemaphoreType.DMA((16,)),
            pltpu.SemaphoreType.DMA((MAX_COPIES,)),
            pltpu.SemaphoreType.DMA((MAX_COPIES,)),
        ],
        compiler_params=pltpu.CompilerParams(collective_id=0, has_side_effects=True),
    )(tokens, ln_gain.reshape(1, D), w_key, w_value, queries, head_shift, key_shift)


def solution(mesh):
    placed = (
        P("gr", "tp", "sp", None),
        P(),
        P("sp", None),
        P("sp", None),
        P(("gr", "sp"), None),
        P(),
        P(("gr", "sp"), "tp"),
    )
    return jax.shard_map(
        local,
        mesh=mesh,
        in_specs=placed,
        out_specs=(P(("gr", "sp"), "tp", None), P(("gr", "sp"), None)),
        check_vma=False,
    )
```

time: 157 us -> 51.7 us (0.33)
  waiting for transfers between devices: 57.3 us -> 0 us
  Pallas kernels: 0 us -> 46.5 us
  blocking collectives: 46.2 us -> 0 us
  other arithmetic: 20.9 us -> 0 us
  between operations: 14.2 us -> 0.64 us
  starting transfers between devices: 5.9 us -> 0 us
  local copies, waits for them, and re-layouts: 9.08 us -> 4.43 us
  matrix products: 3.04 us -> 0 us
    pallas_call x0 -> x1, Pallas kernels: none -> 46.5 us  [local(): pl.pallas_call(kernel, out_shape=(jax.ShapeDtypeStruct((1, 2048, 128), BF...]
    all_gather x3 -> x0, blocking collectives: 46.2 us -> none  [the longest x2 30.5 us: stacked_from(): pieces = lax.all_gather(pieces, axes[k], axis=0, tiled=True)]
    all_gather x2 -> x0, waiting for transfers between devices: 43.9 us -> none  [stacked_from(): pieces = lax.all_gather(pieces, axes[k], axis=0, tiled=True)]
    all_to_all x1 -> x0, waiting for transfers between devices: 13.4 us -> none  [local(): lax.all_to_all(arranged, SP, split_axis=0, concat_axis=1, tiled=True)]
    another operation x3 -> x0, other arithmetic: 10.1 us -> none
    all_to_all x1 -> x0, starting transfers between devices: 5.82 us -> none  [local(): lax.all_to_all(arranged, SP, split_axis=0, concat_axis=1, tiled=True)]
    convert_element_type x3 -> x0, other arithmetic: 5.16 us -> none  [the longest x1 4.3 us: local(): (centred * lax.rsqrt(row_var + epsilon) * ln_gain.astype(jnp.float32)).as...]
    reduce_sum x5 -> x0, other arithmetic: 5.03 us -> none  [the longest x1 3.44 us: local(): row_mean = jnp.mean(flat_rows, axis=1, keepdims=True)]
  transfers between devices with their start and end apart: 3 -> 0, of which waited for: 3 -> 0; matrix products, arithmetic and copies ran while one was open for 9% -> 0% of each run, Pallas kernels for 0% -> 0%
where the time goes in v1:
time: 51.7 us; the launch traced here: 51.5 us
  Pallas kernels  46.5 us (90%)
  local copies, waits for them, and re-layouts  4.43 us (9%)
  between operations  0.64 us (1%)
    pallas_call x1, Pallas kernels, local(): pl.pallas_call(kernel, out_shape=(jax.ShapeDtypeStruct((1, 2048, 128), BF...  46.5 us
    unnamed x2, local copies, waits for them, and re-layouts  3.12 us
    reshape x1, local copies, waits for them, and re-layouts, local(): ln_gain.reshape(1, D)  1.31 us

profile of v1, /device:TPU:1, one launch (start us, length us, event | category | flops | bytes accessed | tf_op | source)
XLA Modules:
  0.0 51.5 jit_solution(13115795337317949617)
XLA Ops:
  0.6 1.3 %reshape.7.gain_hbm = bf16[1,4096]{1,0:T(2,128)(2,1)} reshape(bf16[4096]{0:T(1024)(128)(2,1)} %param.8) | data formatting | bytes 16384 | tf_op jit(solution)/shard_map/reshape | solution.py:393
  1.9 46.5 %shard_map.86 = (bf16[1,2048,128]{2,1,0:T(8,128)(2,1)}, f32[1,512]{1,0:T(1,128)}) custom-call(bf16[4,1,128,4096]{3,2,1,0:T(8,128)(2,1)} %tok_hbm.1, bf16[1,4096]{1,0:T(2,128)(2,1)} %reshape.7.gain_hbm, bf16[256,256]{1,0:T(8,128)(2,1)} %wk_hbm.1, bf16[256,256]{1,0:T(8,128)(2,1)} %wv_hbm.1, bf16[1,512]{1,0:T(2,128)(2,1)} %q_hbm.1, f32[4,8]{1,0:T(4,128)} %hs_hbm.1, ...), custom_call_target="tpu_custom_call" | custom-call | tf_op jit(solution)/shard_map/pallas_call | solution.py:365
  48.4 1.9 %copy.11 = bf16[1,2048,128]{2,1,0:T(8,128)(2,1)} copy(bf16[1,2048,128]{2,1,0:T(8,128)(2,1)} %get-tuple-element.4) | data formatting | bytes 1048576
  50.3 1.3 %copy.12 = f32[1,512]{1,0:T(1,128)} copy(f32[1,512]{1,0:T(1,128)} %get-tuple-element.5) | data formatting | bytes 4096

commit v2 on v1

--- a/solution.py
+++ b/solution.py
@@ -11,8 +11,13 @@
 F32, BF16 = jnp.float32, jnp.bfloat16
 D, HD, KVH, GROUP = 4096, 64, 4, 8
 EPS = 1e-05
-SPLIT = ((128, 128, 0), (0, 0, 256))
-MAX_COPIES = 112
+SPLIT = (128, 128)
+MAX_COPIES = 128
+
+
+class Line:
+    def __init__(self, c, way, rows):
+        self.c, self.way, self.rows = c, way, rows
 
 
 def kernel(
@@ -32,9 +37,6 @@
 
     def at_y(k):
         return (gr, zl * 4 + (y + k) % 4, tp)
-
-    def at_x(k):
-        return (gr, sp, ((x + k) % 4) * 2 + core)
 
     def at_sp(k):
         return (gr, (sp + k) % 16, tp)
@@ -68,121 +70,90 @@
         locals_.append(copy)
         return copy
 
-    plan = []
+    lines = []
     for c in range(2):
-        a, b, d = SPLIT[c]
-        p = {"c": c, "a": a // 2, "b": b // 2, "d": d // 8}
-        p["a0"] = pl.multiple_of(core * (a // 2), 32)
-        p["b0"] = pl.multiple_of(a + core * (b // 2), 32)
-        p["d0"] = pl.multiple_of(a + b + tp * (d // 8), 16)
-        p["own"] = []
-        for size in ("a", "b", "d"):
-            if p[size]:
-                rows = pl.ds(p[size + "0"], p[size])
-                source = (wk_hbm, wv_hbm)[c].at[rows, :]
-                p["own"].append(fetch(source, w.at[c, zl, y, rows, :]))
-        plan.append(p)
+        first = SPLIT[c]
+        for way, (start, count) in enumerate(((0, first), (first, 256 - first))):
+            if count == 0:
+                continue
+            rows = pl.ds(pl.multiple_of(start + core * (count // 2), 16), count // 2)
+            lines.append(Line(c, way, rows))
+    for line in lines:
+        source = (wk_hbm, wv_hbm)[line.c].at[line.rows, :]
+        line.own = fetch(source, w.at[line.c, zl, y, line.rows, :])
     got_gain = fetch(gain_hbm, gain)
     got_tok = [fetch(tok_hbm.at[s, 0], tok.at[s]) for s in range(4)]
     got_small = [fetch(q_hbm, qv), fetch(hs_hbm, hsv), fetch(ks_hbm, ksv)]
 
     barrier = pltpu.get_barrier_semaphore()
     friends = [at_z(k) for k in (1, -1, 2, -2)]
-    friends += [at_sp(k) for k in range(1, 16)]
+    friends += [at_y(k) for k in (1, -1, 2)]
     friends += [at_tp(k) for k in range(1, 8)]
     for friend in friends:
         pl.semaphore_signal(barrier, inc=1, device_id=friend, device_id_type=MESH)
     pl.semaphore_wait(barrier, len(friends))
 
-    def piece(c, zi, yi, start, count):
-        return w.at[c, zi, yi, pl.ds(start, count), :]
-
-    def both(c, zi, yi, start, count, device):
-        ref = piece(c, zi, yi, start, count)
+    every = pl.ds(0, 4)
+    side = 1 - 2 * core
+
+    def shift(line, i, j):
+        mine = (zl, y) if line.way == 0 else (y, zl)
+        return tuple(
+            v if k is None else v if isinstance(k, int) and k == 0 else (v + k + 4) % 4
+            for v, k in zip(mine, (i, j))
+        )
+
+    def pass_on(line, i, j, device):
+        a, b = (every if k is None else v for k, v in zip((i, j), shift(line, i, j)))
+        if line.way == 1:
+            a, b = b, a
+        ref = w.at[line.c, a, b, line.rows, :]
         return send(ref, ref, device)
 
-    every = pl.ds(0, 4)
-    low, high = pl.ds(0, 2), pl.ds(2, 2)
-
-    def stage1(p):
-        c = p["c"]
-        p["s1"] = []
-        if p["a"]:
-            for k in (1, -1, 2 - 4 * core):
-                p["s1"].append(both(c, zl, y, p["a0"], p["a"], at_z(k)))
-        if p["b"]:
-            for k in (1, -1, 2):
-                p["s1"].append(both(c, zl, y, p["b0"], p["b"], at_y(k)))
-        if p["d"]:
-            for k in range(1, 16):
-                p["s1"].append(both(c, zl, y, p["d0"], p["d"], at_sp(k)))
-
-    def stage2(p):
-        c = p["c"]
-        for copy in p["s1"]:
+    def one(line, k):
+        return at_z(k) if line.way == 0 else at_y(k)
+
+    def two(line, k):
+        return at_y(k) if line.way == 0 else at_z(k)
+
+    def wave0(line):
+        line.own.wait()
+        far = 2 * side if line.way == 0 else 2
+        line.far = pass_on(line, 0, 0, one(line, far))
+        line.near = [pass_on(line, 0, 0, one(line, k)) for k in (1, -1)]
+        line.side = {0: [pass_on(line, 0, 0, two(line, k)) for k in (1, -1)]}
+
+    def wave1(line):
+        for copy, i in zip(line.near, (-1, 1)):
             copy.wait_recv()
-        p["s2"], p["pair"] = [], []
-        if p["a"]:
-            for k in (1, -1):
-                p["s2"].append(both(c, every, y, p["a0"], p["a"], at_y(k)))
-        if p["b"]:
-            for k in (1, -1):
-                p["s2"].append(both(c, zl, every, p["b0"], p["b"], at_z(k)))
-        if p["d"]:
-            for k in (1, -1):
-                p["s2"].append(both(c, every, every, p["d0"], p["d"], at_x(k)))
-        if p["a"]:
-            p["pair"].append(both(c, every, y, p["a0"], p["a"], sibling))
-        if p["b"]:
-            p["pair"].append(both(c, zl, every, p["b0"], p["b"], sibling))
-        if p["d"]:
-            p["pair"].append(both(c, every, every, p["d0"], p["d"], sibling))
-
-    def stage3(p):
-        c = p["c"]
-        for copy in p["s2"]:
+            line.side[i] = [pass_on(line, i, 0, two(line, k)) for k in (1, -1)]
+
+    def wave2(line):
+        line.far.wait_recv()
+        line.side[2] = [pass_on(line, 2, 0, two(line, k)) for k in (1, -1)]
+        line.pair = [pass_on(line, None, 0, sibling)]
+
+    def wave3(line):
+        line.relay = []
+        for i in (0, -1, 1):
+            for copy in line.side[i]:
+                copy.wait_recv()
+            way = side if i == 0 else -side
+            line.relay.append(pass_on(line, i, -way, two(line, way)))
+
+    def wave4(line):
+        for copy in line.side[2]:
             copy.wait_recv()
-        p["s3"] = []
-        up, down = (y + 1) % 4, (y + 3) % 4
-        zup, zdown = (zl + 1) % 4, (zl + 3) % 4
-        xup, xdown = (x + 1) % 4, (x + 3) % 4
-        if p["a"]:
-            p["s3"].append(both(c, low, down, p["a0"], p["a"], at_y(1)))
-            p["s3"].append(both(c, high, up, p["a0"], p["a"], at_y(-1)))
-        if p["b"]:
-            p["s3"].append(both(c, zdown, low, p["b0"], p["b"], at_z(1)))
-            p["s3"].append(both(c, zup, high, p["b0"], p["b"], at_z(-1)))
-        if p["d"]:
-            base = p["d0"] - tp * p["d"]
-            first = pl.multiple_of(base + (xdown * 2 + core) * p["d"], 16)
-            second = pl.multiple_of(base + (xup * 2 + core) * p["d"], 16)
-            p["s3"].append(both(c, low, every, first, p["d"], at_x(1)))
-            p["s3"].append(both(c, high, every, second, p["d"], at_x(-1)))
-        if p["a"]:
-            for side in (down, up):
-                p["pair"].append(both(c, every, side, p["a0"], p["a"], sibling))
-        if p["b"]:
-            for side in (zdown, zup):
-                p["pair"].append(both(c, side, every, p["b0"], p["b"], sibling))
-        if p["d"]:
-            for start in (first, second):
-                p["pair"].append(both(c, every, every, start, p["d"], sibling))
-
-    def stage4(p):
-        c = p["c"]
-        for copy in p["s3"]:
+        line.relay.append(pass_on(line, 2, -side, two(line, side)))
+        line.pair += [pass_on(line, None, k, sibling) for k in (-1, 1)]
+
+    def wave5(line):
+        for copy in line.relay:
             copy.wait_recv()
-        if p["a"]:
-            p["pair"].append(both(c, every, (y + 2) % 4, p["a0"], p["a"], sibling))
-        if p["b"]:
-            p["pair"].append(both(c, (zl + 2) % 4, every, p["b0"], p["b"], sibling))
-        if p["d"]:
-            base = p["d0"] - tp * p["d"]
-            start = pl.multiple_of(base + (((x + 2) % 4) * 2 + core) * p["d"], 16)
-            p["pair"].append(both(c, every, every, start, p["d"], sibling))
-
-    def stage5(p):
-        for copy in p["pair"]:
+        line.pair.append(pass_on(line, None, 2, sibling))
+
+    def wave6(line):
+        for copy in line.pair:
             copy.wait_recv()
 
     def norm(s):
@@ -209,7 +180,7 @@
                 out_rows = pl.ds(pl.multiple_of(s * 128 + r, 16), 16)
                 for j in range(32):
                     cols = slice(j * 128, (j + 1) * 128)
-                    value = (tile(j) - mean) * scale * gain[:, cols].astype(F32)
+                    value = (tile(j) - mean) * scale * gain[cols].astype(F32).reshape(1, 128)
                     nrm[out_rows, cols] = value.astype(BF16)
             return carry
 
@@ -242,25 +213,33 @@
             out.append(send(kvs.at[c, far[1]], kvr.at[c, sp], far))
         return out
 
-    for p in plan:
-        for copy in p["own"]:
-            copy.wait()
-    stage1(plan[0])
-    stage1(plan[1])
+    k_lines = [line for line in lines if line.c == 0]
+    v_lines = [line for line in lines if line.c == 1]
+
+    def each(wave, some):
+        for line in some:
+            wave(line)
+
+    each(wave0, k_lines)
+    each(wave0, v_lines)
     got_gain.wait()
     norm(0)
-    stage2(plan[0])
+    each(wave1, k_lines)
     norm(1)
-    stage2(plan[1])
+    each(wave2, k_lines)
+    each(wave1, v_lines)
     norm(2)
-    stage3(plan[0])
+    each(wave3, k_lines)
+    each(wave2, v_lines)
     norm(3)
-    stage4(plan[0])
-    stage3(plan[1])
-    stage5(plan[0])
+    each(wave4, k_lines)
+    each(wave3, v_lines)
+    each(wave5, k_lines)
+    each(wave4, v_lines)
+    each(wave6, k_lines)
     moved_k = project(0)
-    stage4(plan[1])
-    stage5(plan[1])
+    each(wave5, v_lines)
+    each(wave6, v_lines)
     moved_v = project(1)
 
     for copy in got_small:
@@ -378,7 +357,7 @@
             pltpu.VMEM((2, 16, 64, 128), BF16),
             pltpu.VMEM((2, 16, 64, 128), BF16),
             pltpu.VMEM((2048, 128), BF16),
-            pltpu.VMEM((1, D), BF16),
+            pltpu.VMEM((D,), BF16),
             pltpu.VMEM((1, 512), BF16),
             pltpu.VMEM((4, 8), F32),
             pltpu.VMEM((1, 2048), F32),
@@ -390,7 +369,7 @@
             pltpu.SemaphoreType.DMA((MAX_COPIES,)),
         ],
         compiler_params=pltpu.CompilerParams(collective_id=0, has_side_effects=True),
-    )(tokens, ln_gain.reshape(1, D), w_key, w_value, queries, head_shift, key_shift)
+    )(tokens, ln_gain, w_key, w_value, queries, head_shift, key_shift)
 
 
 def solution(mesh):

time: 51.7 us -> 49 us (0.948)
  Pallas kernels: 46.5 us -> 45.1 us
  local copies, waits for them, and re-layouts: 4.43 us -> 3.12 us
    pallas_call x1, Pallas kernels: 46.5 us -> 45.1 us  [local(): pl.pallas_call(kernel, out_shape=(jax.ShapeDtypeStruct((1, 2048, 128), BF...]
    reshape x1 -> x0, local copies, waits for them, and re-layouts: 1.31 us -> none  [local(): ln_gain.reshape(1, D)]
where the time goes in v2:
time: 49 us; the launch traced here: 48.8 us
  Pallas kernels  45.1 us (92%)
  local copies, waits for them, and re-layouts  3.12 us (6%)
  between operations  0.64 us (1%)
    pallas_call x1, Pallas kernels, local(): pl.pallas_call(kernel, out_shape=(jax.ShapeDtypeStruct((1, 2048, 128), BF...  45.1 us
    unnamed x2, local copies, waits for them, and re-layouts  3.12 us

profile of v2, /device:TPU:1, one launch (start us, length us, event | category | flops | bytes accessed | tf_op | source)
XLA Modules:
  0.0 48.8 jit_solution(4116570656534572285)
XLA Ops:
  0.6 45.1 %shard_map.86 = (bf16[1,2048,128]{2,1,0:T(8,128)(2,1)}, f32[1,512]{1,0:T(1,128)}) custom-call(bf16[4,1,128,4096]{3,2,1,0:T(8,128)(2,1)} %tok_hbm.1, bf16[4096]{0:T(1024)(128)(2,1)} %gain_hbm.1, bf16[256,256]{1,0:T(8,128)(2,1)} %wk_hbm.1, bf16[256,256]{1,0:T(8,128)(2,1)} %wv_hbm.1, bf16[1,512]{1,0:T(2,128)(2,1)} %q_hbm.1, f32[4,8]{1,0:T(4,128)} %hs_hbm.1, ...), custom_call_target="tpu_custom_call" | custom-call | tf_op jit(solution)/shard_map/pallas_call | solution.py:344
  45.7 1.9 %copy.11 = bf16[1,2048,128]{2,1,0:T(8,128)(2,1)} copy(bf16[1,2048,128]{2,1,0:T(8,128)(2,1)} %get-tuple-element.4) | data formatting | bytes 1048576
  47.6 1.3 %copy.12 = f32[1,512]{1,0:T(1,128)} copy(f32[1,512]{1,0:T(1,128)} %get-tuple-element.5) | data formatting | bytes 4096

commit v3 on v2

--- a/solution.py
+++ b/solution.py
@@ -12,19 +12,23 @@
 D, HD, KVH, GROUP = 4096, 64, 4, 8
 EPS = 1e-05
 SPLIT = (128, 128)
-MAX_COPIES = 128
+LINES, PER_LINE = 4, 7
+NEAR, FAR, SECOND, PAIR, SENT = 0, 1, (2, 3, 4), 5, 6
+BLOCKS, BLOCKS_SENT = LINES * PER_LINE, LINES * PER_LINE + 2
+SHARED, SHARED_SENT = BLOCKS + 4, BLOCKS + 5
+SEMAPHORES = BLOCKS + 6
 
 
 class Line:
-    def __init__(self, c, way, rows):
-        self.c, self.way, self.rows = c, way, rows
+    def __init__(self, number, c, way, rows):
+        self.number, self.c, self.way, self.rows = number, c, way, rows
 
 
 def kernel(
     tok_hbm, gain_hbm, wk_hbm, wv_hbm, q_hbm, hs_hbm, ks_hbm,
     cache_hbm, read_hbm,
     tok, nrm, w, acc, kvs, kvr, cache, gain, qv, hsv, ksv, rdv, xs, xr,
-    local_sem, send_sem, recv_sem,
+    ruler, local_sem, sems,
 ):
     gr, sp, tp = lax.axis_index("gr"), lax.axis_index("sp"), lax.axis_index("tp")
     x, core = tp // 2, tp % 2
@@ -46,21 +50,19 @@
 
     sibling = (gr, sp, x * 2 + 1 - core)
 
-    copies = []
-
-    def send(src, dst, device):
-        number = len(copies)
-        copy = pltpu.make_async_remote_copy(
+    def send(src, dst, device, sent, arrived):
+        pltpu.make_async_remote_copy(
             src_ref=src,
             dst_ref=dst,
-            send_sem=send_sem.at[number],
-            recv_sem=recv_sem.at[number],
+            send_sem=sems.at[sent],
+            recv_sem=sems.at[arrived],
             device_id=device,
             device_id_type=MESH,
-        )
-        copy.start()
-        copies.append(copy)
-        return copy
+        ).start()
+
+    def take(number, kib):
+        span = ruler.at[pl.ds(0, kib * 4), :]
+        pltpu.make_async_copy(span, span, sems.at[number]).wait()
 
     locals_ = []
 
@@ -72,12 +74,10 @@
 
     lines = []
     for c in range(2):
-        first = SPLIT[c]
-        for way, (start, count) in enumerate(((0, first), (first, 256 - first))):
-            if count == 0:
-                continue
-            rows = pl.ds(pl.multiple_of(start + core * (count // 2), 16), count // 2)
-            lines.append(Line(c, way, rows))
+        for way in range(2):
+            start = pl.multiple_of(way * SPLIT[0] + core * (SPLIT[way] // 2), 32)
+            lines.append(Line(len(lines), c, way, pl.ds(start, SPLIT[way] // 2)))
+            lines[-1].kib = SPLIT[way] // 4
     for line in lines:
         source = (wk_hbm, wv_hbm)[line.c].at[line.rows, :]
         line.own = fetch(source, w.at[line.c, zl, y, line.rows, :])
@@ -97,64 +97,61 @@
     side = 1 - 2 * core
 
     def shift(line, i, j):
-        mine = (zl, y) if line.way == 0 else (y, zl)
+        mine = (y, zl) if line.way == 1 else (zl, y)
         return tuple(
             v if k is None else v if isinstance(k, int) and k == 0 else (v + k + 4) % 4
             for v, k in zip(mine, (i, j))
         )
 
-    def pass_on(line, i, j, device):
+    def pass_on(line, i, j, device, kind):
         a, b = (every if k is None else v for k, v in zip((i, j), shift(line, i, j)))
         if line.way == 1:
             a, b = b, a
         ref = w.at[line.c, a, b, line.rows, :]
-        return send(ref, ref, device)
+        base = line.number * PER_LINE
+        send(ref, ref, device, base + SENT, base + kind)
+
+    def arrived(line, kind, pieces):
+        take(line.number * PER_LINE + kind, pieces * line.kib)
 
     def one(line, k):
-        return at_z(k) if line.way == 0 else at_y(k)
+        return at_y(k) if line.way == 1 else at_z(k)
 
     def two(line, k):
-        return at_y(k) if line.way == 0 else at_z(k)
+        return at_z(k) if line.way == 1 else at_y(k)
+
+    def offsets(along_z):
+        return (2 * side if along_z else 2, 1, -1)
+
+    def along(line, i):
+        for k, kind in zip(offsets(line.way == 1), SECOND):
+            pass_on(line, i, 0, two(line, k), kind)
 
     def wave0(line):
         line.own.wait()
-        far = 2 * side if line.way == 0 else 2
-        line.far = pass_on(line, 0, 0, one(line, far))
-        line.near = [pass_on(line, 0, 0, one(line, k)) for k in (1, -1)]
-        line.side = {0: [pass_on(line, 0, 0, two(line, k)) for k in (1, -1)]}
+        for k, kind in zip(offsets(line.way == 0), (FAR, NEAR, NEAR)):
+            pass_on(line, 0, 0, one(line, k), kind)
 
     def wave1(line):
-        for copy, i in zip(line.near, (-1, 1)):
-            copy.wait_recv()
-            line.side[i] = [pass_on(line, i, 0, two(line, k)) for k in (1, -1)]
+        along(line, 0)
 
     def wave2(line):
-        line.far.wait_recv()
-        line.side[2] = [pass_on(line, 2, 0, two(line, k)) for k in (1, -1)]
-        line.pair = [pass_on(line, None, 0, sibling)]
+        arrived(line, NEAR, 2)
+        along(line, -1)
+        along(line, 1)
 
     def wave3(line):
-        line.relay = []
-        for i in (0, -1, 1):
-            for copy in line.side[i]:
-                copy.wait_recv()
-            way = side if i == 0 else -side
-            line.relay.append(pass_on(line, i, -way, two(line, way)))
+        arrived(line, FAR, 1)
+        along(line, 2)
+        pass_on(line, None, 0, sibling, PAIR)
 
     def wave4(line):
-        for copy in line.side[2]:
-            copy.wait_recv()
-        line.relay.append(pass_on(line, 2, -side, two(line, side)))
-        line.pair += [pass_on(line, None, k, sibling) for k in (-1, 1)]
+        for n, j in ((1, -1), (2, 1), (0, 2)):
+            arrived(line, SECOND[n], 4)
+            pass_on(line, None, j, sibling, PAIR)
 
     def wave5(line):
-        for copy in line.relay:
-            copy.wait_recv()
-        line.pair.append(pass_on(line, None, 2, sibling))
-
-    def wave6(line):
-        for copy in line.pair:
-            copy.wait_recv()
+        arrived(line, PAIR, 16)
 
     def norm(s):
         got_tok[s].wait()
@@ -207,11 +204,9 @@
                 kvs[c, s * 4 + 2 * p] = even.astype(BF16)
                 kvs[c, s * 4 + 2 * p + 1] = odd.astype(BF16)
         kvr[c, sp] = kvs[c, sp]
-        out = []
         for k in range(1, 16):
             far = at_sp(k)
-            out.append(send(kvs.at[c, far[1]], kvr.at[c, sp], far))
-        return out
+            send(kvs.at[c, far[1]], kvr.at[c, sp], far, BLOCKS_SENT + c, BLOCKS + c)
 
     k_lines = [line for line in lines if line.c == 0]
     v_lines = [line for line in lines if line.c == 1]
@@ -221,26 +216,24 @@
             wave(line)
 
     each(wave0, k_lines)
-    each(wave0, v_lines)
     got_gain.wait()
     norm(0)
     each(wave1, k_lines)
+    each(wave2, k_lines)
+    each(wave3, k_lines)
+    each(wave0, v_lines)
     norm(1)
-    each(wave2, k_lines)
     each(wave1, v_lines)
     norm(2)
-    each(wave3, k_lines)
     each(wave2, v_lines)
     norm(3)
+    each(wave3, v_lines)
     each(wave4, k_lines)
-    each(wave3, v_lines)
     each(wave5, k_lines)
+    project(0)
     each(wave4, v_lines)
-    each(wave6, k_lines)
-    moved_k = project(0)
     each(wave5, v_lines)
-    each(wave6, v_lines)
-    moved_v = project(1)
+    project(1)
 
     for copy in got_small:
         copy.wait()
@@ -260,8 +253,7 @@
     eye = lax.broadcasted_iota(jnp.int32, (8, 8), 0) == lax.broadcasted_iota(jnp.int32, (8, 8), 1)
     head = jnp.sum(jnp.where(eye, jnp.broadcast_to(own, (8, 8)), 0.0), axis=1, keepdims=True)
 
-    for copy in moved_k:
-        copy.wait_recv()
+    take(BLOCKS, 240)
     logits = lax.dot_general(
         stack, kvr[0].reshape(1024, 128), (((1,), (1,)), ((), ())), preferred_element_type=F32
     )
@@ -298,14 +290,14 @@
         [jnp.concatenate(w_lo, axis=1), jnp.concatenate(w_hi, axis=1)], axis=0
     ).astype(BF16)
 
-    for copy in moved_v:
-        copy.wait_recv()
+    take(BLOCKS + 1, 240)
     out = jnp.dot(wstack, kvr[1].reshape(1024, 128), preferred_element_type=F32)
     section = out[:8] + turn(out[8:])
     message = jnp.where(left8, section, tail)
     xs[...] = message
     xr[tp] = message
-    shared = [send(xs, xr.at[tp], at_tp(k)) for k in range(1, 8)]
+    for k in range(1, 8):
+        send(xs, xr.at[tp], at_tp(k), SHARED_SENT, SHARED)
 
     def assemble(j, carry):
         keys = kvr[0, j].astype(F32)
@@ -319,8 +311,7 @@
     lax.fori_loop(0, 16, assemble, 0)
     stored = fetch(cache, cache_hbm.at[0])
 
-    for copy in shared:
-        copy.wait_recv()
+    take(SHARED, 28)
     carry = jnp.zeros((8, 128), F32)
     result = jnp.zeros((8, 128), F32)
     for t in reversed(range(8)):
@@ -333,8 +324,11 @@
             left8[:1], result[2 * k : 2 * k + 1], result[2 * k + 1 : 2 * k + 2]
         )
     answered = fetch(rdv, read_hbm)
-    for copy in copies:
-        copy.wait_send()
+    for line in lines:
+        take(line.number * PER_LINE + SENT, 31 * line.kib)
+    for c in range(2):
+        take(BLOCKS_SENT + c, 240)
+    take(SHARED_SENT, 28)
     stored.wait()
     answered.wait()
 
@@ -364,9 +358,9 @@
             pltpu.VMEM((1, 512), F32),
             pltpu.VMEM((8, 128), F32),
             pltpu.VMEM((8, 8, 128), F32),
-            pltpu.SemaphoreType.DMA((16,)),
-            pltpu.SemaphoreType.DMA((MAX_COPIES,)),
-            pltpu.SemaphoreType.DMA((MAX_COPIES,)),
+            pltpu.VMEM((4096, 128), BF16),
+            pltpu.SemaphoreType.DMA((14,)),
+            pltpu.SemaphoreType.DMA((SEMAPHORES,)),
         ],
         compiler_params=pltpu.CompilerParams(collective_id=0, has_side_effects=True),
     )(tokens, ln_gain, w_key, w_value, queries, head_shift, key_shift)

time: 49 us -> 47.8 us (0.976)
  Pallas kernels: 45.1 us -> 43.9 us
    pallas_call x1, Pallas kernels: 45.1 us -> 43.9 us  [local(): pl.pallas_call(kernel, out_shape=(jax.ShapeDtypeStruct((1, 2048, 128), BF...]
where the time goes in v3:
time: 47.8 us; the launch traced here: 47.6 us
  Pallas kernels  43.9 us (92%)
  local copies, waits for them, and re-layouts  3.12 us (7%)
  between operations  0.64 us (1%)
    pallas_call x1, Pallas kernels, local(): pl.pallas_call(kernel, out_shape=(jax.ShapeDtypeStruct((1, 2048, 128), BF...  43.9 us
    unnamed x2, local copies, waits for them, and re-layouts  3.12 us

profile of v3, /device:TPU:1, one launch (start us, length us, event | category | flops | bytes accessed | tf_op | source)
XLA Modules:
  0.0 47.6 jit_solution(16114091430510047807)
XLA Ops:
  0.6 43.9 %shard_map.86 = (bf16[1,2048,128]{2,1,0:T(8,128)(2,1)}, f32[1,512]{1,0:T(1,128)}) custom-call(bf16[4,1,128,4096]{3,2,1,0:T(8,128)(2,1)} %tok_hbm.1, bf16[4096]{0:T(1024)(128)(2,1)} %gain_hbm.1, bf16[256,256]{1,0:T(8,128)(2,1)} %wk_hbm.1, bf16[256,256]{1,0:T(8,128)(2,1)} %wv_hbm.1, bf16[1,512]{1,0:T(2,128)(2,1)} %q_hbm.1, f32[4,8]{1,0:T(4,128)} %hs_hbm.1, ...), custom_call_target="tpu_custom_call" | custom-call | tf_op jit(solution)/shard_map/pallas_call | solution.py:338
  44.5 1.9 %copy.11 = bf16[1,2048,128]{2,1,0:T(8,128)(2,1)} copy(bf16[1,2048,128]{2,1,0:T(8,128)(2,1)} %get-tuple-element.4) | data formatting | bytes 1048576
  46.4 1.3 %copy.12 = f32[1,512]{1,0:T(1,128)} copy(f32[1,512]{1,0:T(1,128)} %get-tuple-element.5) | data formatting | bytes 4096

commit v4 on v3

--- a/solution.py
+++ b/solution.py
@@ -216,18 +216,18 @@
             wave(line)
 
     each(wave0, k_lines)
+    each(wave0, v_lines)
     got_gain.wait()
     norm(0)
     each(wave1, k_lines)
     each(wave2, k_lines)
     each(wave3, k_lines)
-    each(wave0, v_lines)
+    each(wave1, v_lines)
+    each(wave2, v_lines)
+    each(wave3, v_lines)
     norm(1)
-    each(wave1, v_lines)
     norm(2)
-    each(wave2, v_lines)
     norm(3)
-    each(wave3, v_lines)
     each(wave4, k_lines)
     each(wave5, k_lines)
     project(0)

time: 47.8 us -> 46.2 us (0.967)
  Pallas kernels: 43.9 us -> 42.3 us
    pallas_call x1, Pallas kernels: 43.9 us -> 42.3 us  [local(): pl.pallas_call(kernel, out_shape=(jax.ShapeDtypeStruct((1, 2048, 128), BF...]
where the time goes in v4:
time: 46.2 us; the launch traced here: 46.1 us
  Pallas kernels  42.3 us (92%)
  local copies, waits for them, and re-layouts  3.12 us (7%)
  between operations  0.64 us (1%)
    pallas_call x1, Pallas kernels, local(): pl.pallas_call(kernel, out_shape=(jax.ShapeDtypeStruct((1, 2048, 128), BF...  42.3 us
    unnamed x2, local copies, waits for them, and re-layouts  3.12 us

profile of v4, /device:TPU:1, one launch (start us, length us, event | category | flops | bytes accessed | tf_op | source)
XLA Modules:
  0.0 46.1 jit_solution(72567765552876524)
XLA Ops:
  0.6 42.3 %shard_map.86 = (bf16[1,2048,128]{2,1,0:T(8,128)(2,1)}, f32[1,512]{1,0:T(1,128)}) custom-call(bf16[4,1,128,4096]{3,2,1,0:T(8,128)(2,1)} %tok_hbm.1, bf16[4096]{0:T(1024)(128)(2,1)} %gain_hbm.1, bf16[256,256]{1,0:T(8,128)(2,1)} %wk_hbm.1, bf16[256,256]{1,0:T(8,128)(2,1)} %wv_hbm.1, bf16[1,512]{1,0:T(2,128)(2,1)} %q_hbm.1, f32[4,8]{1,0:T(4,128)} %hs_hbm.1, ...), custom_call_target="tpu_custom_call" | custom-call | tf_op jit(solution)/shard_map/pallas_call | solution.py:338
  42.9 1.9 %copy.11 = bf16[1,2048,128]{2,1,0:T(8,128)(2,1)} copy(bf16[1,2048,128]{2,1,0:T(8,128)(2,1)} %get-tuple-element.4) | data formatting | bytes 1048576
  44.8 1.3 %copy.12 = f32[1,512]{1,0:T(1,128)} copy(f32[1,512]{1,0:T(1,128)} %get-tuple-element.5) | data formatting | bytes 4096

commit v5 on v4

--- a/solution.py
+++ b/solution.py
@@ -12,8 +12,8 @@
 D, HD, KVH, GROUP = 4096, 64, 4, 8
 EPS = 1e-05
 SPLIT = (128, 128)
-LINES, PER_LINE = 4, 7
-NEAR, FAR, SECOND, PAIR, SENT = 0, 1, (2, 3, 4), 5, 6
+LINES, PER_LINE = 4, 8
+NEAR, FAR, SECOND, PAIR, SENT, LATE = 0, 1, (2, 3, 4), 5, 6, 7
 BLOCKS, BLOCKS_SENT = LINES * PER_LINE, LINES * PER_LINE + 2
 SHARED, SHARED_SENT = BLOCKS + 4, BLOCKS + 5
 SEMAPHORES = BLOCKS + 6
@@ -26,8 +26,8 @@
 
 def kernel(
     tok_hbm, gain_hbm, wk_hbm, wv_hbm, q_hbm, hs_hbm, ks_hbm,
-    cache_hbm, read_hbm,
-    tok, nrm, w, acc, kvs, kvr, cache, gain, qv, hsv, ksv, rdv, xs, xr,
+    cache_hbm, xr,
+    tok, nrm, w, acc, kvs, kvr, cache, gain, qv, hsv, ksv, xs,
     ruler, local_sem, sems,
 ):
     gr, sp, tp = lax.axis_index("gr"), lax.axis_index("sp"), lax.axis_index("tp")
@@ -125,7 +125,7 @@
 
     def along(line, i):
         for k, kind in zip(offsets(line.way == 1), SECOND):
-            pass_on(line, i, 0, two(line, k), kind)
+            pass_on(line, i, 0, two(line, k), LATE if i == 2 else kind)
 
     def wave0(line):
         line.own.wait()
@@ -147,8 +147,14 @@
 
     def wave4(line):
         for n, j in ((1, -1), (2, 1), (0, 2)):
-            arrived(line, SECOND[n], 4)
-            pass_on(line, None, j, sibling, PAIR)
+            arrived(line, SECOND[n], 3)
+            for i in (0, -1, 1):
+                pass_on(line, i, j, sibling, PAIR)
+
+    def wave6(line):
+        arrived(line, LATE, 3)
+        for j in (-1, 1, 2):
+            pass_on(line, 2, j, sibling, PAIR)
 
     def wave5(line):
         arrived(line, PAIR, 16)
@@ -227,11 +233,13 @@
     each(wave3, v_lines)
     norm(1)
     norm(2)
+    each(wave4, k_lines)
     norm(3)
-    each(wave4, k_lines)
+    each(wave6, k_lines)
     each(wave5, k_lines)
     project(0)
     each(wave4, v_lines)
+    each(wave6, v_lines)
     each(wave5, v_lines)
     project(1)
 
@@ -295,7 +303,7 @@
     section = out[:8] + turn(out[8:])
     message = jnp.where(left8, section, tail)
     xs[...] = message
-    xr[tp] = message
+    kept = fetch(xs, xr.at[tp])
     for k in range(1, 8):
         send(xs, xr.at[tp], at_tp(k), SHARED_SENT, SHARED)
 
@@ -312,6 +320,29 @@
     stored = fetch(cache, cache_hbm.at[0])
 
     take(SHARED, 28)
+    for line in lines:
+        take(line.number * PER_LINE + SENT, 31 * line.kib)
+    for c in range(2):
+        take(BLOCKS_SENT + c, 240)
+    take(SHARED_SENT, 28)
+    stored.wait()
+    kept.wait()
+
+
+def write_out(cache_in, shared_in, cache_out, read_out, cache, xr, rdv, sems):
+    shared = pltpu.make_async_copy(shared_in, xr, sems.at[0, 4])
+    shared.start()
+    ways = [
+        tuple(ref.at[pl.ds(k * 512, 512)] for ref in (cache_in.at[0], cache, cache_out.at[0]))
+        for k in range(4)
+    ]
+    reads = [pltpu.make_async_copy(a, b, sems.at[0, n]) for n, (a, b, _) in enumerate(ways)]
+    writes = [pltpu.make_async_copy(b, c, sems.at[1, n]) for n, (_, b, c) in enumerate(ways)]
+    for copy in reads:
+        copy.start()
+    left8 = lax.broadcasted_iota(jnp.int32, (8, 128), 1) < HD
+    turn = lambda v: pltpu.roll(v, HD, 1)
+    shared.wait()
     carry = jnp.zeros((8, 128), F32)
     result = jnp.zeros((8, 128), F32)
     for t in reversed(range(8)):
@@ -323,23 +354,23 @@
         rdv[:, k * 128 : (k + 1) * 128] = jnp.where(
             left8[:1], result[2 * k : 2 * k + 1], result[2 * k + 1 : 2 * k + 2]
         )
-    answered = fetch(rdv, read_hbm)
-    for line in lines:
-        take(line.number * PER_LINE + SENT, 31 * line.kib)
-    for c in range(2):
-        take(BLOCKS_SENT + c, 240)
-    take(SHARED_SENT, 28)
-    stored.wait()
+    answered = pltpu.make_async_copy(rdv, read_out, sems.at[1, 4])
+    answered.start()
+    for before, after in zip(reads, writes):
+        before.wait()
+        after.start()
+    for copy in writes:
+        copy.wait()
     answered.wait()
 
 
 def local(tokens, ln_gain, w_key, w_value, queries, head_shift, key_shift):
     any_ = pl.BlockSpec(memory_space=pl.ANY)
-    return pl.pallas_call(
+    cache, shared = pl.pallas_call(
         kernel,
         out_shape=(
             jax.ShapeDtypeStruct((1, 2048, 128), BF16),
-            jax.ShapeDtypeStruct((1, 512), F32),
+            jax.ShapeDtypeStruct((8, 8, 128), F32),
         ),
         in_specs=[any_] * 7,
         out_specs=(any_, any_),
@@ -355,15 +386,28 @@
             pltpu.VMEM((1, 512), BF16),
             pltpu.VMEM((4, 8), F32),
             pltpu.VMEM((1, 2048), F32),
-            pltpu.VMEM((1, 512), F32),
             pltpu.VMEM((8, 128), F32),
-            pltpu.VMEM((8, 8, 128), F32),
             pltpu.VMEM((4096, 128), BF16),
             pltpu.SemaphoreType.DMA((14,)),
             pltpu.SemaphoreType.DMA((SEMAPHORES,)),
         ],
         compiler_params=pltpu.CompilerParams(collective_id=0, has_side_effects=True),
     )(tokens, ln_gain, w_key, w_value, queries, head_shift, key_shift)
+    return pl.pallas_call(
+        write_out,
+        out_shape=(
+            jax.ShapeDtypeStruct((1, 2048, 128), BF16),
+            jax.ShapeDtypeStruct((1, 512), F32),
+        ),
+        in_specs=[any_] * 2,
+        out_specs=(any_, any_),
+        scratch_shapes=[
+            pltpu.VMEM((2048, 128), BF16),
+            pltpu.VMEM((8, 8, 128), F32),
+            pltpu.VMEM((1, 512), F32),
+            pltpu.SemaphoreType.DMA((2, 5)),
+        ],
+    )(cache, shared)
 
 
 def solution(mesh):

time: 46.2 us -> 43.7 us (0.946)
  local copies, waits for them, and re-layouts: 3.12 us -> 0 us
  Pallas kernels: 42.3 us -> 42.9 us
    unnamed x2 -> x0, local copies, waits for them, and re-layouts: 3.12 us -> none
    pallas_call x0 -> x1, Pallas kernels: none -> 1.86 us  [local(): pl.pallas_call(write_out, out_shape=(jax.ShapeDtypeStruct((1, 2048, 128),...]
    pallas_call x1, Pallas kernels: 42.3 us -> 41.1 us  [local(): pl.pallas_call(kernel, out_shape=(jax.ShapeDtypeStruct((1, 2048, 128), BF...]
where the time goes in v5:
time: 43.7 us; the launch traced here: 43.6 us
  Pallas kernels  42.9 us (98%)
  between operations  0.64 us (1%)
    pallas_call x1, Pallas kernels, local(): pl.pallas_call(kernel, out_shape=(jax.ShapeDtypeStruct((1, 2048, 128), BF...  41.1 us
    pallas_call x1, Pallas kernels, local(): pl.pallas_call(write_out, out_shape=(jax.ShapeDtypeStruct((1, 2048, 128),...  1.86 us

profile of v5, /device:TPU:1, one launch (start us, length us, event | category | flops | bytes accessed | tf_op | source)
XLA Modules:
  0.0 43.6 jit_solution(18387108843505820349)
XLA Ops:
  0.6 41.1 %shard_map.86 = (bf16[1,2048,128]{2,1,0:T(8,128)(2,1)}, f32[8,8,128]{2,1,0:T(8,128)}) custom-call(bf16[4,1,128,4096]{3,2,1,0:T(8,128)(2,1)} %tok_hbm.1, bf16[4096]{0:T(1024)(128)(2,1)} %gain_hbm.1, bf16[256,256]{1,0:T(8,128)(2,1)} %wk_hbm.1, bf16[256,256]{1,0:T(8,128)(2,1)} %wv_hbm.1, bf16[1,512]{1,0:T(2,128)(2,1)} %q_hbm.1, f32[4,8]{1,0:T(4,128)} %hs_hbm.1, ...), custom_call_target="tpu_custom_call" | custom-call | tf_op jit(solution)/shard_map/pallas_call | solution.py:369
  41.7 1.9 %shard_map.87 = (bf16[1,2048,128]{2,1,0:T(8,128)(2,1)}, f32[1,512]{1,0:T(1,128)}) custom-call(bf16[1,2048,128]{2,1,0:T(8,128)(2,1)} %get-tuple-element.4.cache_in, f32[8,8,128]{2,1,0:T(8,128)} %get-tuple-element.5.shared_in), custom_call_target="tpu_custom_call" | custom-call | tf_op jit(solution)/shard_map/pallas_call | solution.py:396

commit v6 on v5

--- a/solution.py
+++ b/solution.py
@@ -17,6 +17,7 @@
 BLOCKS, BLOCKS_SENT = LINES * PER_LINE, LINES * PER_LINE + 2
 SHARED, SHARED_SENT = BLOCKS + 4, BLOCKS + 5
 SEMAPHORES = BLOCKS + 6
+GROUPS = ((2, 3), (1, 0))
 
 
 class Line:
@@ -71,6 +72,13 @@
         copy.start()
         locals_.append(copy)
         return copy
+
+    barrier = pltpu.get_barrier_semaphore()
+    friends = [at_z(k) for k in (1, -1, 2, -2)]
+    friends += [at_y(k) for k in (1, -1, 2)]
+    friends += [at_tp(k) for k in range(1, 8)]
+    for friend in friends:
+        pl.semaphore_signal(barrier, inc=1, device_id=friend, device_id_type=MESH)
 
     lines = []
     for c in range(2):
@@ -85,12 +93,6 @@
     got_tok = [fetch(tok_hbm.at[s, 0], tok.at[s]) for s in range(4)]
     got_small = [fetch(q_hbm, qv), fetch(hs_hbm, hsv), fetch(ks_hbm, ksv)]
 
-    barrier = pltpu.get_barrier_semaphore()
-    friends = [at_z(k) for k in (1, -1, 2, -2)]
-    friends += [at_y(k) for k in (1, -1, 2)]
-    friends += [at_tp(k) for k in range(1, 8)]
-    for friend in friends:
-        pl.semaphore_signal(barrier, inc=1, device_id=friend, device_id_type=MESH)
     pl.semaphore_wait(barrier, len(friends))
 
     every = pl.ds(0, 4)
@@ -197,22 +199,29 @@
         return pltpu.roll(v, HD, 1)
 
     def project(c):
-        acc[...] = jnp.dot(
-            nrm[...], w[c].reshape(D, 256), preferred_element_type=F32
-        )
-        for s in range(4):
-            for p in range(2):
-                cols = slice(p * 128, (p + 1) * 128)
-                top = acc[s * 128 : s * 128 + 64, cols]
-                bottom = acc[s * 128 + 64 : s * 128 + 128, cols]
-                even = jnp.where(left, top, turn(bottom))
-                odd = jnp.where(left, turn(top), bottom)
-                kvs[c, s * 4 + 2 * p] = even.astype(BF16)
-                kvs[c, s * 4 + 2 * p + 1] = odd.astype(BF16)
-        kvr[c, sp] = kvs[c, sp]
-        for k in range(1, 16):
-            far = at_sp(k)
-            send(kvs.at[c, far[1]], kvr.at[c, sp], far, BLOCKS_SENT + c, BLOCKS + c)
+        weights = w[c].reshape(D, 256)
+        for group in GROUPS:
+            starts = [(zl + o) % 4 for o in group]
+            rows = [nrm[pl.ds(pl.multiple_of(s * 128, 128), 128), :] for s in starts]
+            acc[: len(group) * 128] = jnp.dot(
+                jnp.concatenate(rows, axis=0), weights, preferred_element_type=F32
+            )
+            for n, (o, s) in enumerate(zip(group, starts)):
+                for p in range(2):
+                    cols = slice(p * 128, (p + 1) * 128)
+                    top = acc[n * 128 : n * 128 + 64, cols]
+                    bottom = acc[n * 128 + 64 : n * 128 + 128, cols]
+                    even = jnp.where(left, top, turn(bottom))
+                    odd = jnp.where(left, turn(top), bottom)
+                    kvs[c, s * 4 + 2 * p] = even.astype(BF16)
+                    kvs[c, s * 4 + 2 * p + 1] = odd.astype(BF16)
+                for k in range(4):
+                    far = s * 4 + (y + k) % 4
+                    if o or k:
+                        device = (gr, far, tp)
+                        send(kvs.at[c, far], kvr.at[c, sp], device, BLOCKS_SENT + c, BLOCKS + c)
+                    else:
+                        kvr[c, sp] = kvs[c, sp]
 
     k_lines = [line for line in lines if line.c == 0]
     v_lines = [line for line in lines if line.c == 1]

time: 43.7 us -> 43.5 us (level)
  no operation moved by 1% of the time
where the time goes in v6:
time: 43.5 us; the launch traced here: 43.4 us
  Pallas kernels  42.8 us (98%)
  between operations  0.64 us (1%)
    pallas_call x1, Pallas kernels, local(): pl.pallas_call(kernel, out_shape=(jax.ShapeDtypeStruct((1, 2048, 128), BF...  40.9 us
    pallas_call x1, Pallas kernels, local(): pl.pallas_call(write_out, out_shape=(jax.ShapeDtypeStruct((1, 2048, 128),...  1.86 us

profile of v6, /device:TPU:1, one launch (start us, length us, event | category | flops | bytes accessed | tf_op | source)
XLA Modules:
  0.0 43.4 jit_solution(16484420573959558531)
XLA Ops:
  0.6 40.9 %shard_map.86 = (bf16[1,2048,128]{2,1,0:T(8,128)(2,1)}, f32[8,8,128]{2,1,0:T(8,128)}) custom-call(bf16[4,1,128,4096]{3,2,1,0:T(8,128)(2,1)} %tok_hbm.1, bf16[4096]{0:T(1024)(128)(2,1)} %gain_hbm.1, bf16[256,256]{1,0:T(8,128)(2,1)} %wk_hbm.1, bf16[256,256]{1,0:T(8,128)(2,1)} %wv_hbm.1, bf16[1,512]{1,0:T(2,128)(2,1)} %q_hbm.1, f32[4,8]{1,0:T(4,128)} %hs_hbm.1, ...), custom_call_target="tpu_custom_call" | custom-call | tf_op jit(solution)/shard_map/pallas_call | solution.py:378
  41.5 1.9 %shard_map.87 = (bf16[1,2048,128]{2,1,0:T(8,128)(2,1)}, f32[1,512]{1,0:T(1,128)}) custom-call(bf16[1,2048,128]{2,1,0:T(8,128)(2,1)} %get-tuple-element.4.cache_in, f32[8,8,128]{2,1,0:T(8,128)} %get-tuple-element.5.shared_in), custom_call_target="tpu_custom_call" | custom-call | tf_op jit(solution)/shard_map/pallas_call | solution.py:405

commit v7 on v6

--- a/solution.py
+++ b/solution.py
@@ -131,7 +131,7 @@
 
     def wave0(line):
         line.own.wait()
-        for k, kind in zip(offsets(line.way == 0), (FAR, NEAR, NEAR)):
+        for k, kind in reversed(list(zip(offsets(line.way == 0), (FAR, NEAR, NEAR)))):
             pass_on(line, 0, 0, one(line, k), kind)
 
     def wave1(line):
@@ -232,9 +232,9 @@
 
     each(wave0, k_lines)
     each(wave0, v_lines)
+    each(wave1, k_lines)
     got_gain.wait()
     norm(0)
-    each(wave1, k_lines)
     each(wave2, k_lines)
     each(wave3, k_lines)
     each(wave1, v_lines)

time: 43.5 us -> 43.6 us (level)
  no operation moved by 1% of the time
where the time goes in v7:
time: 43.6 us; the launch traced here: 43.5 us
  Pallas kernels  42.8 us (98%)
  between operations  0.64 us (1%)
    pallas_call x1, Pallas kernels, local(): pl.pallas_call(kernel, out_shape=(jax.ShapeDtypeStruct((1, 2048, 128), BF...  41 us
    pallas_call x1, Pallas kernels, local(): pl.pallas_call(write_out, out_shape=(jax.ShapeDtypeStruct((1, 2048, 128),...  1.86 us

profile of v7, /device:TPU:1, one launch (start us, length us, event | category | flops | bytes accessed | tf_op | source)
XLA Modules:
  0.0 43.5 jit_solution(11300378831288832887)
XLA Ops:
  0.6 41.0 %shard_map.86 = (bf16[1,2048,128]{2,1,0:T(8,128)(2,1)}, f32[8,8,128]{2,1,0:T(8,128)}) custom-call(bf16[4,1,128,4096]{3,2,1,0:T(8,128)(2,1)} %tok_hbm.1, bf16[4096]{0:T(1024)(128)(2,1)} %gain_hbm.1, bf16[256,256]{1,0:T(8,128)(2,1)} %wk_hbm.1, bf16[256,256]{1,0:T(8,128)(2,1)} %wv_hbm.1, bf16[1,512]{1,0:T(2,128)(2,1)} %q_hbm.1, f32[4,8]{1,0:T(4,128)} %hs_hbm.1, ...), custom_call_target="tpu_custom_call" | custom-call | tf_op jit(solution)/shard_map/pallas_call | solution.py:378
  41.6 1.9 %shard_map.87 = (bf16[1,2048,128]{2,1,0:T(8,128)(2,1)}, f32[1,512]{1,0:T(1,128)}) custom-call(bf16[1,2048,128]{2,1,0:T(8,128)(2,1)} %get-tuple-element.4.cache_in, f32[8,8,128]{2,1,0:T(8,128)} %get-tuple-element.5.shared_in), custom_call_target="tpu_custom_call" | custom-call | tf_op jit(solution)/shard_map/pallas_call | solution.py:405
